TPU v7x, 256 devices: a whole 4x4x8 slice. The times are simulated.
256 devices in a mesh: kv: 32 (over z, y), tp: 8 (over x, core).
Axes of the slice: x: 4, y: 4, z: 8, core: 2. Of those that a mesh axis runs over, the one named last changes fastest.
Arguments:
- residual_in: bfloat16 [256, 2048], P(None, ('kv', 'tp')), may hold values from -14 to 14
- delta_state: float32 [256, 32, 128, 128], P('kv', 'tp'), may hold values from -1 to 1
- norm_gain_first: float32 [2048], P('kv'), may hold values from 0.1 to 1.9
- gate_first: bfloat16 [2048, 5632], P('kv', 'tp'), may hold values from -0.125 to 0.125
- up_first: bfloat16 [2048, 5632], P('kv', 'tp'), may hold values from -0.125 to 0.125
- down_first: bfloat16 [5632, 2048], P('tp', 'kv'), may hold values from -0.15625 to 0.15625
- norm_gain_mixer: float32 [2048], P('kv'), may hold values from 0.1 to 1.9
- query_weight: bfloat16 [2048, 2048], P('kv', 'tp'), may hold values from -0.125 to 0.125
- key_weight: bfloat16 [2048, 2048], P('kv', 'tp'), may hold values from -0.125 to 0.125
- value_weight: bfloat16 [2048, 4096], P('kv', 'tp'), may hold values from -0.125 to 0.125
- output_gate_weight: bfloat16 [2048, 4096], P('kv', 'tp'), may hold values from -0.125 to 0.125
- beta_weight: bfloat16 [2048, 32], P('kv'), may hold values from -0.125 to 0.125
- decay_weight: bfloat16 [2048, 32], P('kv'), may hold values from -0.125 to 0.125
- decay_rate: float32 [32], P('tp'), may hold values from -2.3 to 1.1
- decay_bias: float32 [32], P('tp'), may hold values from -1 to 1
- head_gain: float32 [128], replicated, may hold values from 0.1 to 1.9
- out_weight: bfloat16 [4096, 2048], P('tp', 'kv'), may hold values from -0.125 to 0.125
- norm_gain_second: float32 [2048], P('kv'), may hold values from 0.1 to 1.9
- gate_second: bfloat16 [2048, 5632], P('kv', 'tp'), may hold values from -0.125 to 0.125
- up_second: bfloat16 [2048, 5632], P('kv', 'tp'), may hold values from -0.125 to 0.125
- down_second: bfloat16 [5632, 2048], P('tp', 'kv'), may hold values from -0.15625 to 0.15625
Outputs:
- residual_out: bfloat16 [256, 2048], P(None, ('kv', 'tp'))
- delta_state_out: float32 [256, 32, 128, 128], P('kv', 'tp')
All inputs are finite; a program needn't handle non-finite values.
Results may differ from a plain program's by a relative error of at most 0.03.
Values may be sent and summed in bfloat16 or wider, within the bound.
A program may use at most 64 MiB of HBM per device.

v0:
```python
import jax
import jax.numpy as jnp
from jax import lax
from jax.sharding import PartitionSpec as P

D = 2048
epsilon = 1e-06


def in_blocks(value, dim, size):
    before, after = (value.shape[:dim], value.shape[dim + 1 :])
    return jnp.moveaxis(value.reshape(*before, size, -1, *after), dim, 0)


def summed_on_arrival(value, axis, dim):
    blocks = in_blocks(value, dim, lax.axis_size(axis))
    arrived = lax.all_to_all(blocks, axis, split_axis=0, concat_axis=0, tiled=True)
    return arrived.astype(jnp.float32).sum(axis=0)


def side_by_side(arrays, axis, dim, along):
    columns = [a.reshape(*a.shape[:along], -1) for a in arrays]
    both = jnp.concatenate(columns, axis=along)
    result, at, outs = (summed_on_arrival(both, axis, dim), 0, [])
    for a, column in zip(arrays, columns):
        piece = result[..., at : at + column.shape[along]]
        outs.append(piece.reshape(*piece.shape[:along], *a.shape[along:]))
        at += column.shape[along]
    return tuple(outs)


def joined_along(blocks, dim):
    dims = list(blocks.shape[1:])
    dims[dim] *= blocks.shape[0]
    return jnp.moveaxis(blocks, 0, dim).reshape(dims)


def from_everyone(value, axis):
    copies = jnp.broadcast_to(value, (lax.axis_size(axis), *value.shape))
    return lax.all_to_all(copies, axis, split_axis=0, concat_axis=0, tiled=True)


def collect(value, axis, dim):
    return joined_along(from_everyone(value, axis), dim)


def activate(summed, square_sums, hidden_cols):
    rowscale = lax.rsqrt(square_sums / D + epsilon)[:, None]
    gate_act = summed[:, :hidden_cols] * rowscale
    up_act = summed[:, hidden_cols:] * rowscale
    return (jax.nn.silu(gate_act) * up_act).astype(jnp.bfloat16)


def feed_forward(residual, norm_gain, gate_weight, up_weight, down_weight, finish):
    as_float = residual.astype(jnp.float32)
    squares = jnp.sum(as_float * as_float, axis=1)
    scaled = (as_float * norm_gain).astype(jnp.bfloat16)
    joined = jnp.concatenate([gate_weight, up_weight], axis=1)
    partial_value = jnp.dot(scaled, joined, preferred_element_type=jnp.float32)
    hidden_cols = gate_weight.shape[1]
    summed, square_sums = side_by_side(
        (partial_value.astype(jnp.bfloat16), squares.astype(jnp.bfloat16)), "kv", 0, 1
    )
    hidden = activate(summed, square_sums, hidden_cols)
    projected = jnp.dot(
        collect(hidden, "kv", 0), down_weight, preferred_element_type=jnp.float32
    ).astype(jnp.bfloat16)
    if finish:
        col_count = residual.shape[1] // lax.axis_size("tp")
        own_cols = lax.dynamic_slice_in_dim(
            as_float, lax.axis_index("tp") * col_count, col_count, 1
        )
        branch = summed_on_arrival(projected, "tp", 1)
        return (own_cols + 0.5 * branch).astype(jnp.bfloat16)
    branch = lax.psum(projected, "tp").astype(jnp.float32)
    return (as_float + 0.5 * branch).astype(jnp.bfloat16)


def unit_heads(projected, head_size):
    activated = jax.nn.silu(projected).reshape(projected.shape[0], -1, head_size)
    return activated * lax.rsqrt(jnp.sum(activated * activated, axis=-1, keepdims=True) + epsilon)


def delta_step(old_state, key_rows, queries, values, beta_gate, decay_gate):
    faded_state = old_state * decay_gate[:, :, None, None]
    predicted = jnp.einsum("rhab,rha->rhb", faded_state, key_rows, precision=lax.Precision.HIGHEST)
    correction = beta_gate[:, :, None] * (values - predicted)
    updated = faded_state + key_rows[:, :, :, None] * correction[:, :, None, :]
    reading = jnp.einsum("rhab,rha->rhb", updated, queries, precision=lax.Precision.HIGHEST)
    return (updated, reading)


def token_mixer(
    residual,
    norm_gain,
    query_weight,
    key_weight,
    value_weight,
    output_gate_weight,
    beta_weight,
    decay_weight,
    decay_rate,
    decay_bias,
    head_gain,
    out_weight,
    old_state,
):
    as_float = residual.astype(jnp.float32)
    squares = jnp.sum(as_float * as_float, axis=1)
    scaled = (as_float * norm_gain).astype(jnp.bfloat16)
    joined = jnp.concatenate([query_weight, key_weight, value_weight, output_gate_weight], axis=1)
    partial_value = jnp.dot(scaled, joined, preferred_element_type=jnp.float32)
    heads_dev = decay_rate.shape[0]
    head_start = lax.axis_index("tp") * heads_dev
    gate_cols = jnp.concatenate(
        [
            lax.dynamic_slice_in_dim(beta_weight, head_start, heads_dev, 1),
            lax.dynamic_slice_in_dim(decay_weight, head_start, heads_dev, 1),
        ],
        axis=1,
    )
    gate_part = jnp.dot(scaled, gate_cols, preferred_element_type=jnp.float32)
    row_count = old_state.shape[0]
    summed, gate_summed, square_sums = side_by_side(
        (
            partial_value.astype(jnp.bfloat16),
            gate_part.astype(jnp.bfloat16),
            squares.astype(jnp.bfloat16),
        ),
        "kv",
        0,
        1,
    )
    rowscale = lax.rsqrt(square_sums / D + epsilon)[:, None]
    summed = summed * rowscale
    gate_summed = gate_summed * rowscale
    head_size = old_state.shape[2]
    key_cols = query_weight.shape[1]
    value_cols = value_weight.shape[1]
    repeat_count = heads_dev // (key_cols // head_size)
    queries = jnp.repeat(
        unit_heads(summed[:, :key_cols], head_size) * head_size ** (-0.5), repeat_count, axis=1
    )
    key_rows = jnp.repeat(
        unit_heads(summed[:, key_cols : 2 * key_cols], head_size), repeat_count, axis=1
    )
    values = jax.nn.silu(summed[:, 2 * key_cols : 2 * key_cols + value_cols]).reshape(
        row_count, heads_dev, head_size
    )
    out_gate = jax.nn.silu(summed[:, 2 * key_cols + value_cols :]).reshape(
        row_count, heads_dev, head_size
    )
    beta_gate = jax.nn.sigmoid(gate_summed[:, :heads_dev])
    decay_gate = jnp.exp(
        -jnp.exp(decay_rate)[None, :]
        * jax.nn.softplus(gate_summed[:, heads_dev:] + decay_bias[None, :])
    )
    new_state, reading = delta_step(old_state, key_rows, queries, values, beta_gate, decay_gate)
    normed = reading * lax.rsqrt(jnp.mean(reading * reading, axis=-1, keepdims=True) + epsilon)
    normed = (
        (normed * head_gain * out_gate)
        .reshape(row_count, heads_dev * head_size)
        .astype(jnp.bfloat16)
    )
    projected = jnp.dot(
        collect(normed, "kv", 0), out_weight, preferred_element_type=jnp.float32
    ).astype(jnp.bfloat16)
    branch = lax.psum(projected, "tp").astype(jnp.float32)
    return ((as_float + branch).astype(jnp.bfloat16), new_state)


def body(
    residual_in,
    delta_state,
    norm_gain_first,
    gate_first,
    up_first,
    down_first,
    norm_gain_mixer,
    query_weight,
    key_weight,
    value_weight,
    output_gate_weight,
    beta_weight,
    decay_weight,
    decay_rate,
    decay_bias,
    head_gain,
    out_weight,
    norm_gain_second,
    gate_second,
    up_second,
    down_second,
):
    columns = lax.all_gather(residual_in, "tp", axis=1, tiled=True)
    after_first = feed_forward(columns, norm_gain_first, gate_first, up_first, down_first, False)
    after_mixer, new_state = token_mixer(
        after_first,
        norm_gain_mixer,
        query_weight,
        key_weight,
        value_weight,
        output_gate_weight,
        beta_weight,
        decay_weight,
        decay_rate,
        decay_bias,
        head_gain,
        out_weight,
        delta_state,
    )
    residual_out = feed_forward(
        after_mixer, norm_gain_second, gate_second, up_second, down_second, True
    )
    return (residual_out, new_state)


def solution(mesh):
    placed = (
        P(None, ("kv", "tp")),
        P("kv", "tp", None, None),
        P("kv"),
        P("kv", "tp"),
        P("kv", "tp"),
        P("tp", "kv"),
        P("kv"),
        P("kv", "tp"),
        P("kv", "tp"),
        P("kv", "tp"),
        P("kv", "tp"),
        P("kv", None),
        P("kv", None),
        P("tp"),
        P("tp"),
        P(),
        P("tp", "kv"),
        P("kv"),
        P("kv", "tp"),
        P("kv", "tp"),
        P("tp", "kv"),
    )
    return jax.shard_map(
        body,
        mesh=mesh,
        in_specs=placed,
        out_specs=(P(None, ("kv", "tp")), P("kv", "tp", None, None)),
        check_vma=False,
    )
```

profile of v0, /device:TPU:1, one launch (start us, length us, event | category | flops | bytes accessed | tf_op | source)
XLA Modules:
  0.0 230.6 jit_solution(4892839816095156955)
XLA Ops:
  0.6 16.2 %all_gather.3 = bf16[256,64]{0,1:T(8,128)(2,1)S(1)} all-gather(bf16[256,8]{0,1:T(8,128)(2,1)} %param.21), channel_id=1, replica_groups=mesh['kv'=32,'tp'=8] {'tp'}, dimensions={1}, use_global_device_ids=true | all-gather | bytes 36864 | tf_op jit(solution)/shard_map/all_gather | solution.py:195
  16.9 0.2 convert_element_type.152
  17.1 1.4 fusion
  18.7 31.4 %all_to_all.35 = bf16[32,8,1409]{2,1,0:T(8,128)(2,1)S(1)} all-to-all(bf16[32,8,1409]{2,1,0:T(8,128)(2,1)S(1)} %pad_maximum_fusion), channel_id=1, replica_groups=mesh['kv'=32,'tp'=8] {'kv'}, dimensions={0} | all-to-all | bytes 1442816 | tf_op jit(solution)/shard_map/all_to_all | solution.py:17
  50.4 0.8 broadcast_in_dim.10
  51.2 5.6 %all-to-all-start.1 = ((bf16[32,8,704]{2,1,0:T(8,128)(2,1)}), bf16[32,8,704]{2,1,0:T(8,128)(2,1)S(1)}, u32[]{:S(2)}, u32[]{:S(2)}) async-start(bf16[32,8,704]{2,1,0:T(8,128)(2,1)} %broadcast_in_dim.10), calls=%async_computation.1 | async-start | bytes 786432 | tf_op jit(solution)/shard_map/all_to_all | solution.py:40
  56.8 0.7 constant_dynamic-slice_fusion
  57.5 12.1 %all-to-all-done.1 = bf16[32,8,704]{2,1,0:T(8,128)(2,1)S(1)} async-done(((bf16[32,8,704]{2,1,0:T(8,128)(2,1)}), bf16[32,8,704]{2,1,0:T(8,128)(2,1)S(1)}, u32[]{:S(2)}, u32[]{:S(2)}) %all-to-all-start.1) | async-done | bytes 360480 | tf_op jit(solution)/shard_map/all_to_all | solution.py:40
  69.6 0.2 convolution_convert_fusion.5
  69.8 23.5 %psum.14 = bf16[256,64]{0,1:T(8,128)(2,1)S(1)} all-reduce(bf16[256,64]{0,1:T(8,128)(2,1)S(1)} %convolution_convert_fusion.5), channel_id=1, replica_groups=mesh['kv'=32,'tp'=8] {'tp'}, use_global_device_ids=true, to_apply=%region_2.3 | all-reduce | flops 16384 | bytes 65536 | tf_op jit(solution)/shard_map/psum | solution.py:75
  93.4 0.2 convolution_convert_fusion.6
  93.7 0.2 convert_element_type.153
  94.0 0.5 fusion.1
  94.5 1.1 concatenate.39
  95.6 4.6 %all-to-all-start.2 = ((bf16[32,8,1545]{2,1,0:T(8,128)(2,1)}), bf16[32,8,1545]{2,1,0:T(8,128)(2,1)S(1)}, u32[]{:S(2)}, u32[]{:S(2)}) async-start(bf16[32,8,1545]{2,1,0:T(8,128)(2,1)} %concatenate.39), calls=%async_computation.2 | async-start | bytes 1703936 | tf_op jit(solution)/shard_map/all_to_all | solution.py:17
  100.3 19.5 %all-to-all-done.2 = bf16[32,8,1545]{2,1,0:T(8,128)(2,1)S(1)} async-done(((bf16[32,8,1545]{2,1,0:T(8,128)(2,1)}), bf16[32,8,1545]{2,1,0:T(8,128)(2,1)S(1)}, u32[]{:S(2)}, u32[]{:S(2)}) %all-to-all-start.2) | async-done | bytes 791072 | tf_op jit(solution)/shard_map/all_to_all | solution.py:17
  119.8 0.2 fusion.54
  120.6 2.0 fusion.3
  122.7 0.7 multiply_add_fusion
  123.6 1.2 copy-done.2
  124.8 1.9 fusion.67
  126.9 17.3 %all_to_all.36 = bf16[32,8,512]{2,1,0:T(8,128)(2,1)S(1)} all-to-all(bf16[32,8,512]{2,1,0:T(8,128)(2,1)S(1)} %broadcast_in_dim.13), channel_id=1, replica_groups=mesh['kv'=32,'tp'=8] {'kv'}, dimensions={0} | all-to-all | bytes 524288 | tf_op jit(solution)/shard_map/all_to_all | solution.py:40
  144.2 0.2 convolution_convert_fusion.3
  144.4 26.0 %psum.15 = bf16[256,64]{0,1:T(8,128)(2,1)S(1)} all-reduce(bf16[256,64]{0,1:T(8,128)(2,1)S(1)} %convolution_convert_fusion.3), channel_id=1, replica_groups=mesh['kv'=32,'tp'=8] {'tp'}, use_global_device_ids=true, to_apply=%region_8.9 | all-reduce | flops 16384 | bytes 65536 | tf_op jit(solution)/shard_map/psum | solution.py:168
  170.4 0.2 convert_element_type.154
  170.7 0.5 fusion.2
  171.2 22.8 %all_to_all.37 = bf16[32,8,1409]{2,1,0:T(8,128)(2,1)S(1)} all-to-all(bf16[32,8,1409]{2,1,0:T(8,128)(2,1)S(1)} %pad_maximum_fusion.1), channel_id=1, replica_groups=mesh['kv'=32,'tp'=8] {'kv'}, dimensions={0} | all-to-all | bytes 1442816 | tf_op jit(solution)/shard_map/all_to_all | solution.py:17
  194.4 18.7 %all_to_all.38 = bf16[32,8,704]{2,1,0:T(8,128)(2,1)S(1)} all-to-all(bf16[32,8,704]{2,1,0:T(8,128)(2,1)S(1)} %broadcast_in_dim.14), channel_id=1, replica_groups=mesh['kv'=32,'tp'=8] {'kv'}, dimensions={0} | all-to-all | bytes 720896 | tf_op jit(solution)/shard_map/all_to_all | solution.py:40
  213.1 0.9 fusion.5
  214.0 11.3 %all-to-all-start.6 = ((bf16[8,256,8]{1,2,0:T(8,128)(2,1)}), bf16[8,256,8]{1,2,0:T(8,128)(2,1)S(1)}, u32[]{:S(2)}, u32[]{:S(2)}) async-start(bf16[8,256,8]{1,2,0:T(8,128)(2,1)} %fusion.5), calls=%async_computation.6 | async-start | bytes 65536 | tf_op jit(solution)/shard_map/all_to_all | solution.py:17
  225.2 4.7 %all-to-all-done.6 = bf16[8,256,8]{1,2,0:T(8,128)(2,1)S(1)} async-done(((bf16[8,256,8]{1,2,0:T(8,128)(2,1)}), bf16[8,256,8]{1,2,0:T(8,128)(2,1)S(1)}, u32[]{:S(2)}, u32[]{:S(2)}) %all-to-all-start.6) | async-done | bytes 32800 | tf_op jit(solution)/shard_map/all_to_all | solution.py:17
  230.0 0.6 add_convert_fusion
  (65 shorter events, 2.1 us)
Async XLA Ops:
  0.6 68.9 %copy-start = (bf16[704,64]{0,1:T(8,128)(2,1)S(1)}, bf16[704,64]{0,1:T(8,128)(2,1)}, u32[]{:S(2)}) copy-start(bf16[704,64]{0,1:T(8,128)(2,1)} %param.26) | copy-start | bytes 270340
  18.6 74.8 %copy-start.11 = (f32[64]{0:T(128)S(1)}, f32[64]{0:T(128)}, u32[]{:S(2)}) copy-start(f32[64]{0:T(128)} %param.27) | copy-start | bytes 772
  18.6 75.4 %copy-start.6 = (bf16[64,512]{1,0:T(8,128)(2,1)S(1)}, bf16[64,512]{1,0:T(8,128)(2,1)}, u32[]{:S(2)}) copy-start(bf16[64,512]{1,0:T(8,128)(2,1)} %param.31) | copy-start | bytes 196612
  18.6 75.4 %copy-start.7 = (bf16[64,512]{1,0:T(8,128)(2,1)S(1)}, bf16[64,512]{1,0:T(8,128)(2,1)}, u32[]{:S(2)}) copy-start(bf16[64,512]{1,0:T(8,128)(2,1)} %param.30) | copy-start | bytes 196612
  18.6 75.4 %copy-start.9 = (bf16[64,256]{1,0:T(8,128)(2,1)S(1)}, bf16[64,256]{1,0:T(8,128)(2,1)}, u32[]{:S(2)}) copy-start(bf16[64,256]{1,0:T(8,128)(2,1)} %param.29) | copy-start | bytes 98308
  18.7 75.4 %copy-start.10 = (bf16[64,256]{1,0:T(8,128)(2,1)S(1)}, bf16[64,256]{1,0:T(8,128)(2,1)}, u32[]{:S(2)}) copy-start(bf16[64,256]{1,0:T(8,128)(2,1)} %param.28) | copy-start | bytes 98308
  51.2 18.4 %all-to-all-start.1 = ((bf16[32,8,704]{2,1,0:T(8,128)(2,1)}), bf16[32,8,704]{2,1,0:T(8,128)(2,1)S(1)}, u32[]{:S(2)}, u32[]{:S(2)}) async-start(bf16[32,8,704]{2,1,0:T(8,128)(2,1)} %broadcast_in_dim.10), calls=%async_computation.1 | async-start | bytes 786432 | tf_op jit(solution)/shard_map/all_to_all | solution.py:40
  94.0 6.2 %copy-start.15 = (f32[4]{0:T(128)S(1)}, f32[4]{0:T(128)}, u32[]{:S(2)}) copy-start(f32[4]{0:T(128)} %param.34) | copy-start | bytes 52
  94.5 25.8 %copy-start.14 = (f32[4]{0:T(128)S(1)}, f32[4]{0:T(128)}, u32[]{:S(2)}) copy-start(f32[4]{0:T(128)} %param.35) | copy-start | bytes 52
  94.5 26.1 %copy-start.1 = (f32[8,4,128,128]{3,2,1,0:T(8,128)S(1)}, f32[8,4,128,128]{3,2,1,0:T(8,128)}, u32[]{:S(2)}) copy-start(f32[8,4,128,128]{3,2,1,0:T(8,128)} %param.22) | copy-start | bytes 6291460
  95.6 24.1 %all-to-all-start.2 = ((bf16[32,8,1545]{2,1,0:T(8,128)(2,1)}), bf16[32,8,1545]{2,1,0:T(8,128)(2,1)S(1)}, u32[]{:S(2)}, u32[]{:S(2)}) async-start(bf16[32,8,1545]{2,1,0:T(8,128)(2,1)} %concatenate.39), calls=%async_computation.2 | async-start | bytes 1703936 | tf_op jit(solution)/shard_map/all_to_all | solution.py:17
  123.5 1.3 copy-start.2
  123.5 3.3 %copy-start.13 = (f32[128]{0:T(128)S(1)}, f32[128]{0:T(128)}, u32[]{:S(2)}) copy-start(f32[128]{0:T(128)} %param.36) | copy-start | bytes 1540
  123.5 20.7 %copy-start.8 = (bf16[512,64]{0,1:T(8,128)(2,1)S(1)}, bf16[512,64]{0,1:T(8,128)(2,1)}, u32[]{:S(2)}) copy-start(bf16[512,64]{0,1:T(8,128)(2,1)} %param.37) | copy-start | bytes 196612
  123.5 47.1 %copy-start.3 = (bf16[64,704]{1,0:T(8,128)(2,1)S(1)}, bf16[64,704]{1,0:T(8,128)(2,1)}, u32[]{:S(2)}) copy-start(bf16[64,704]{1,0:T(8,128)(2,1)} %param.40) | copy-start | bytes 270340
  123.5 47.1 %copy-start.4 = (bf16[64,704]{1,0:T(8,128)(2,1)S(1)}, bf16[64,704]{1,0:T(8,128)(2,1)}, u32[]{:S(2)}) copy-start(bf16[64,704]{1,0:T(8,128)(2,1)} %param.39) | copy-start | bytes 270340
  123.5 47.1 %copy-start.12 = (f32[64]{0:T(128)S(1)}, f32[64]{0:T(128)}, u32[]{:S(2)}) copy-start(f32[64]{0:T(128)} %param.38) | copy-start | bytes 772
  171.2 41.9 %copy-start.5 = (bf16[704,64]{0,1:T(8,128)(2,1)S(1)}, bf16[704,64]{0,1:T(8,128)(2,1)}, u32[]{:S(2)}) copy-start(bf16[704,64]{0,1:T(8,128)(2,1)} %param.41) | copy-start | bytes 270340
  214.0 16.0 %all-to-all-start.6 = ((bf16[8,256,8]{1,2,0:T(8,128)(2,1)}), bf16[8,256,8]{1,2,0:T(8,128)(2,1)S(1)}, u32[]{:S(2)}, u32[]{:S(2)}) async-start(bf16[8,256,8]{1,2,0:T(8,128)(2,1)} %fusion.5), calls=%async_computation.6 | async-start | bytes 65536 | tf_op jit(solution)/shard_map/all_to_all | solution.py:17
where the time goes:
time: 231 us
  blocking collectives  156 us (68%)
  waiting for transfers between devices  36.3 us (16%)
  starting transfers between devices  21.5 us (9%)
  matrix products  7.71 us (3%)
  local copies, waits for them, and re-layouts  4.91 us (2%)
  other arithmetic  3.23 us (1%)
    all_to_all x2, blocking collectives, summed_on_arrival(): lax.all_to_all(blocks, axis, split_axis=0, concat_axis=0, tiled=True)  54.2 us
    all_to_all x2, blocking collectives, from_everyone(): return lax.all_to_all(copies, axis, split_axis=0, concat_axis=0, tiled=True)  36 us
    psum x1, blocking collectives, token_mixer(): branch = lax.psum(projected, 'tp').astype(jnp.float32)  26 us
    all_to_all x2, waiting for transfers between devices, summed_on_arrival(): lax.all_to_all(blocks, axis, split_axis=0, concat_axis=0, tiled=True)  24.2 us
    psum x1, blocking collectives, feed_forward(): branch = lax.psum(projected, 'tp').astype(jnp.float32)  23.5 us
    all_gather x1, blocking collectives, body(): columns = lax.all_gather(residual_in, 'tp', axis=1, tiled=True)  16.2 us
    all_to_all x2, starting transfers between devices, summed_on_arrival(): lax.all_to_all(blocks, axis, split_axis=0, concat_axis=0, tiled=True)  15.9 us
    all_to_all x1, waiting for transfers between devices, from_everyone(): return lax.all_to_all(copies, axis, split_axis=0, concat_axis=0, tiled=True)  12.1 us
  transfers between devices with their start and end apart: 3, of which 3 were waited for; matrix products, arithmetic and copies ran while one was open for 0% of the time, Pallas kernels for 0%

commit v1 on v0

--- a/solution.py
+++ b/solution.py
@@ -5,6 +5,12 @@
 
 D = 2048
 epsilon = 1e-06
+
+
+def stack_and_merge(x, mesh_axis, d):
+    terms = lax.all_gather(x, mesh_axis, axis=0, tiled=False)
+    whole = jnp.concatenate(terms, axis=d)
+    return whole
 
 
 def in_blocks(value, dim, size):
@@ -192,7 +198,7 @@
     up_second,
     down_second,
 ):
-    columns = lax.all_gather(residual_in, "tp", axis=1, tiled=True)
+    columns = stack_and_merge(residual_in, "tp", 1)
     after_first = feed_forward(columns, norm_gain_first, gate_first, up_first, down_first, False)
     after_mixer, new_state = token_mixer(
         after_first,

time: 231 us -> 231 us (level)
  no operation moved by 1% of the time
where the time goes in v1:
time: 231 us
  blocking collectives  156 us (68%)
  waiting for transfers between devices  36.3 us (16%)
  starting transfers between devices  21.5 us (9%)
  matrix products  7.71 us (3%)
  local copies, waits for them, and re-layouts  4.91 us (2%)
  other arithmetic  3.23 us (1%)
    all_to_all x2, blocking collectives, summed_on_arrival(): lax.all_to_all(blocks, axis, split_axis=0, concat_axis=0, tiled=True)  54.2 us
    all_to_all x2, blocking collectives, from_everyone(): return lax.all_to_all(copies, axis, split_axis=0, concat_axis=0, tiled=True)  36 us
    psum x1, blocking collectives, token_mixer(): branch = lax.psum(projected, 'tp').astype(jnp.float32)  26 us
    all_to_all x2, waiting for transfers between devices, summed_on_arrival(): lax.all_to_all(blocks, axis, split_axis=0, concat_axis=0, tiled=True)  24.2 us
    psum x1, blocking collectives, feed_forward(): branch = lax.psum(projected, 'tp').astype(jnp.float32)  23.5 us
    all_gather x1, blocking collectives, stack_and_merge(): terms = lax.all_gather(x, mesh_axis, axis=0, tiled=False)  16.2 us
    all_to_all x2, starting transfers between devices, summed_on_arrival(): lax.all_to_all(blocks, axis, split_axis=0, concat_axis=0, tiled=True)  15.9 us
    all_to_all x1, waiting for transfers between devices, from_everyone(): return lax.all_to_all(copies, axis, split_axis=0, concat_axis=0, tiled=True)  12.1 us
  transfers between devices with their start and end apart: 3, of which 3 were waited for; matrix products, arithmetic and copies ran while one was open for 0% of the time, Pallas kernels for 0%

profile of v1, /device:TPU:1, one launch (start us, length us, event | category | flops | bytes accessed | tf_op | source)
XLA Modules:
  0.0 230.6 jit_solution(7465245645543897204)
XLA Ops:
  0.6 16.2 %all-gather = bf16[2048,8]{0,1:T(8,128)(2,1)S(1)} all-gather(bf16[256,8]{0,1:T(8,128)(2,1)} %param.21), channel_id=2, replica_groups=mesh['kv'=32,'tp'=8] {'tp'}, dimensions={0}, use_global_device_ids=true | all-gather | bytes 36864 | tf_op jit(solution)/shard_map/all_gather | solution.py:11
  16.9 0.2 convert_element_type.169
  17.1 1.4 fusion
  18.7 31.4 %all_to_all.35 = bf16[32,8,1409]{2,1,0:T(8,128)(2,1)S(1)} all-to-all(bf16[32,8,1409]{2,1,0:T(8,128)(2,1)S(1)} %pad_maximum_fusion), channel_id=1, replica_groups=mesh['kv'=32,'tp'=8] {'kv'}, dimensions={0} | all-to-all | bytes 1442816 | tf_op jit(solution)/shard_map/all_to_all | solution.py:23
  50.4 0.8 broadcast_in_dim.10
  51.2 5.6 %all-to-all-start.1 = ((bf16[32,8,704]{2,1,0:T(8,128)(2,1)}), bf16[32,8,704]{2,1,0:T(8,128)(2,1)S(1)}, u32[]{:S(2)}, u32[]{:S(2)}) async-start(bf16[32,8,704]{2,1,0:T(8,128)(2,1)} %broadcast_in_dim.10), calls=%async_computation.1 | async-start | bytes 786432 | tf_op jit(solution)/shard_map/all_to_all | solution.py:46
  56.8 0.7 constant_dynamic-slice_fusion
  57.5 12.1 %all-to-all-done.1 = bf16[32,8,704]{2,1,0:T(8,128)(2,1)S(1)} async-done(((bf16[32,8,704]{2,1,0:T(8,128)(2,1)}), bf16[32,8,704]{2,1,0:T(8,128)(2,1)S(1)}, u32[]{:S(2)}, u32[]{:S(2)}) %all-to-all-start.1) | async-done | bytes 360480 | tf_op jit(solution)/shard_map/all_to_all | solution.py:46
  69.6 0.2 convolution_convert_fusion.5
  69.8 23.5 %psum.14 = bf16[256,64]{0,1:T(8,128)(2,1)S(1)} all-reduce(bf16[256,64]{0,1:T(8,128)(2,1)S(1)} %convolution_convert_fusion.5), channel_id=1, replica_groups=mesh['kv'=32,'tp'=8] {'tp'}, use_global_device_ids=true, to_apply=%region_2.3 | all-reduce | flops 16384 | bytes 65536 | tf_op jit(solution)/shard_map/psum | solution.py:81
  93.4 0.2 convolution_convert_fusion.6
  93.7 0.2 convert_element_type.170
  94.0 0.5 fusion.1
  94.5 1.1 concatenate.39
  95.6 4.6 %all-to-all-start.2 = ((bf16[32,8,1545]{2,1,0:T(8,128)(2,1)}), bf16[32,8,1545]{2,1,0:T(8,128)(2,1)S(1)}, u32[]{:S(2)}, u32[]{:S(2)}) async-start(bf16[32,8,1545]{2,1,0:T(8,128)(2,1)} %concatenate.39), calls=%async_computation.2 | async-start | bytes 1703936 | tf_op jit(solution)/shard_map/all_to_all | solution.py:23
  100.3 19.5 %all-to-all-done.2 = bf16[32,8,1545]{2,1,0:T(8,128)(2,1)S(1)} async-done(((bf16[32,8,1545]{2,1,0:T(8,128)(2,1)}), bf16[32,8,1545]{2,1,0:T(8,128)(2,1)S(1)}, u32[]{:S(2)}, u32[]{:S(2)}) %all-to-all-start.2) | async-done | bytes 791072 | tf_op jit(solution)/shard_map/all_to_all | solution.py:23
  119.8 0.2 fusion.56
  120.6 2.0 fusion.3
  122.7 0.7 multiply_add_fusion
  123.6 1.2 copy-done.2
  124.8 1.9 fusion.69
  126.9 17.3 %all_to_all.36 = bf16[32,8,512]{2,1,0:T(8,128)(2,1)S(1)} all-to-all(bf16[32,8,512]{2,1,0:T(8,128)(2,1)S(1)} %broadcast_in_dim.13), channel_id=1, replica_groups=mesh['kv'=32,'tp'=8] {'kv'}, dimensions={0} | all-to-all | bytes 524288 | tf_op jit(solution)/shard_map/all_to_all | solution.py:46
  144.2 0.2 convolution_convert_fusion.3
  144.4 26.0 %psum.15 = bf16[256,64]{0,1:T(8,128)(2,1)S(1)} all-reduce(bf16[256,64]{0,1:T(8,128)(2,1)S(1)} %convolution_convert_fusion.3), channel_id=1, replica_groups=mesh['kv'=32,'tp'=8] {'tp'}, use_global_device_ids=true, to_apply=%region_8.9 | all-reduce | flops 16384 | bytes 65536 | tf_op jit(solution)/shard_map/psum | solution.py:174
  170.4 0.2 convert_element_type.171
  170.7 0.5 fusion.2
  171.2 22.8 %all_to_all.37 = bf16[32,8,1409]{2,1,0:T(8,128)(2,1)S(1)} all-to-all(bf16[32,8,1409]{2,1,0:T(8,128)(2,1)S(1)} %pad_maximum_fusion.1), channel_id=1, replica_groups=mesh['kv'=32,'tp'=8] {'kv'}, dimensions={0} | all-to-all | bytes 1442816 | tf_op jit(solution)/shard_map/all_to_all | solution.py:23
  194.4 18.7 %all_to_all.38 = bf16[32,8,704]{2,1,0:T(8,128)(2,1)S(1)} all-to-all(bf16[32,8,704]{2,1,0:T(8,128)(2,1)S(1)} %broadcast_in_dim.14), channel_id=1, replica_groups=mesh['kv'=32,'tp'=8] {'kv'}, dimensions={0} | all-to-all | bytes 720896 | tf_op jit(solution)/shard_map/all_to_all | solution.py:46
  213.1 0.9 fusion.5
  214.0 11.3 %all-to-all-start.6 = ((bf16[8,256,8]{1,2,0:T(8,128)(2,1)}), bf16[8,256,8]{1,2,0:T(8,128)(2,1)S(1)}, u32[]{:S(2)}, u32[]{:S(2)}) async-start(bf16[8,256,8]{1,2,0:T(8,128)(2,1)} %fusion.5), calls=%async_computation.6 | async-start | bytes 65536 | tf_op jit(solution)/shard_map/all_to_all | solution.py:23
  225.2 4.7 %all-to-all-done.6 = bf16[8,256,8]{1,2,0:T(8,128)(2,1)S(1)} async-done(((bf16[8,256,8]{1,2,0:T(8,128)(2,1)}), bf16[8,256,8]{1,2,0:T(8,128)(2,1)S(1)}, u32[]{:S(2)}, u32[]{:S(2)}) %all-to-all-start.6) | async-done | bytes 32800 | tf_op jit(solution)/shard_map/all_to_all | solution.py:23
  230.0 0.6 add_convert_fusion
  (65 shorter events, 2.1 us)
Async XLA Ops:
  0.6 68.9 %copy-start = (bf16[704,64]{0,1:T(8,128)(2,1)S(1)}, bf16[704,64]{0,1:T(8,128)(2,1)}, u32[]{:S(2)}) copy-start(bf16[704,64]{0,1:T(8,128)(2,1)} %param.26) | copy-start | bytes 270340
  18.6 74.8 %copy-start.11 = (f32[64]{0:T(128)S(1)}, f32[64]{0:T(128)}, u32[]{:S(2)}) copy-start(f32[64]{0:T(128)} %param.27) | copy-start | bytes 772
  18.6 75.4 %copy-start.6 = (bf16[64,512]{1,0:T(8,128)(2,1)S(1)}, bf16[64,512]{1,0:T(8,128)(2,1)}, u32[]{:S(2)}) copy-start(bf16[64,512]{1,0:T(8,128)(2,1)} %param.31) | copy-start | bytes 196612
  18.6 75.4 %copy-start.7 = (bf16[64,512]{1,0:T(8,128)(2,1)S(1)}, bf16[64,512]{1,0:T(8,128)(2,1)}, u32[]{:S(2)}) copy-start(bf16[64,512]{1,0:T(8,128)(2,1)} %param.30) | copy-start | bytes 196612
  18.6 75.4 %copy-start.9 = (bf16[64,256]{1,0:T(8,128)(2,1)S(1)}, bf16[64,256]{1,0:T(8,128)(2,1)}, u32[]{:S(2)}) copy-start(bf16[64,256]{1,0:T(8,128)(2,1)} %param.29) | copy-start | bytes 98308
  18.7 75.4 %copy-start.10 = (bf16[64,256]{1,0:T(8,128)(2,1)S(1)}, bf16[64,256]{1,0:T(8,128)(2,1)}, u32[]{:S(2)}) copy-start(bf16[64,256]{1,0:T(8,128)(2,1)} %param.28) | copy-start | bytes 98308
  51.2 18.4 %all-to-all-start.1 = ((bf16[32,8,704]{2,1,0:T(8,128)(2,1)}), bf16[32,8,704]{2,1,0:T(8,128)(2,1)S(1)}, u32[]{:S(2)}, u32[]{:S(2)}) async-start(bf16[32,8,704]{2,1,0:T(8,128)(2,1)} %broadcast_in_dim.10), calls=%async_computation.1 | async-start | bytes 786432 | tf_op jit(solution)/shard_map/all_to_all | solution.py:46
  94.0 6.2 %copy-start.15 = (f32[4]{0:T(128)S(1)}, f32[4]{0:T(128)}, u32[]{:S(2)}) copy-start(f32[4]{0:T(128)} %param.34) | copy-start | bytes 52
  94.5 25.8 %copy-start.14 = (f32[4]{0:T(128)S(1)}, f32[4]{0:T(128)}, u32[]{:S(2)}) copy-start(f32[4]{0:T(128)} %param.35) | copy-start | bytes 52
  94.5 26.1 %copy-start.1 = (f32[8,4,128,128]{3,2,1,0:T(8,128)S(1)}, f32[8,4,128,128]{3,2,1,0:T(8,128)}, u32[]{:S(2)}) copy-start(f32[8,4,128,128]{3,2,1,0:T(8,128)} %param.22) | copy-start | bytes 6291460
  95.6 24.1 %all-to-all-start.2 = ((bf16[32,8,1545]{2,1,0:T(8,128)(2,1)}), bf16[32,8,1545]{2,1,0:T(8,128)(2,1)S(1)}, u32[]{:S(2)}, u32[]{:S(2)}) async-start(bf16[32,8,1545]{2,1,0:T(8,128)(2,1)} %concatenate.39), calls=%async_computation.2 | async-start | bytes 1703936 | tf_op jit(solution)/shard_map/all_to_all | solution.py:23
  123.5 1.3 copy-start.2
  123.5 3.3 %copy-start.13 = (f32[128]{0:T(128)S(1)}, f32[128]{0:T(128)}, u32[]{:S(2)}) copy-start(f32[128]{0:T(128)} %param.36) | copy-start | bytes 1540
  123.5 20.7 %copy-start.8 = (bf16[512,64]{0,1:T(8,128)(2,1)S(1)}, bf16[512,64]{0,1:T(8,128)(2,1)}, u32[]{:S(2)}) copy-start(bf16[512,64]{0,1:T(8,128)(2,1)} %param.37) | copy-start | bytes 196612
  123.5 47.1 %copy-start.3 = (bf16[64,704]{1,0:T(8,128)(2,1)S(1)}, bf16[64,704]{1,0:T(8,128)(2,1)}, u32[]{:S(2)}) copy-start(bf16[64,704]{1,0:T(8,128)(2,1)} %param.40) | copy-start | bytes 270340
  123.5 47.1 %copy-start.4 = (bf16[64,704]{1,0:T(8,128)(2,1)S(1)}, bf16[64,704]{1,0:T(8,128)(2,1)}, u32[]{:S(2)}) copy-start(bf16[64,704]{1,0:T(8,128)(2,1)} %param.39) | copy-start | bytes 270340
  123.5 47.1 %copy-start.12 = (f32[64]{0:T(128)S(1)}, f32[64]{0:T(128)}, u32[]{:S(2)}) copy-start(f32[64]{0:T(128)} %param.38) | copy-start | bytes 772
  171.2 41.9 %copy-start.5 = (bf16[704,64]{0,1:T(8,128)(2,1)S(1)}, bf16[704,64]{0,1:T(8,128)(2,1)}, u32[]{:S(2)}) copy-start(bf16[704,64]{0,1:T(8,128)(2,1)} %param.41) | copy-start | bytes 270340
  214.0 16.0 %all-to-all-start.6 = ((bf16[8,256,8]{1,2,0:T(8,128)(2,1)}), bf16[8,256,8]{1,2,0:T(8,128)(2,1)S(1)}, u32[]{:S(2)}, u32[]{:S(2)}) async-start(bf16[8,256,8]{1,2,0:T(8,128)(2,1)} %fusion.5), calls=%async_computation.6 | async-start | bytes 65536 | tf_op jit(solution)/shard_map/all_to_all | solution.py:23
